TPU v7x, 512 devices: a whole 4x4x16 slice. The times are simulated.
512 devices in a mesh: sp: 32 (over z, core), tp: 16 (over y, x).
Axes of the slice: x: 4, y: 4, z: 16, core: 2. Of those that a mesh axis runs over, the one named last changes fastest.
Arguments:
- u_val: bfloat16 [8192, 2048], P('sp', 'tp'), may hold values from -6 to 6
- u_gate: bfloat16 [8192, 2048], P('sp', 'tp'), may hold values from -9 to 9
- conv_weight: float32 [31, 2048], P(None, 'tp')
- conv_bias: float32 [2048], P('tp'), may hold values from -3 to 3
- ln_gain: float32 [2048], P('tp'), may hold values from 0.1 to 1.9
- ln_bias: float32 [2048], P('tp'), may hold values from -3 to 3
- proj_weight: bfloat16 [2048, 4096], P(None, 'tp'), may hold values from -0.125 to 0.125
- resid: bfloat16 [8192, 4096], P('sp', 'tp')
- norm_gain: float32 [4096], P('tp'), may hold values from 0.1 to 1.9
- route_ids: int32 [8192, 2], P('sp'), may hold values from 0 to 31, all different within a row; in each aligned block of 256 rows (0 to 255, 256 to 511, ...) at most 32 rows name the same one
- route_wts: float32 [8192, 2], P('sp'), may hold values from 0.3 to 1.5
- expert_gate: bfloat16 [32, 4096, 1024], P('sp', None, 'tp'), may hold values from -0.09375 to 0.09375
- expert_up: bfloat16 [32, 4096, 1024], P('sp', None, 'tp'), may hold values from -0.09375 to 0.09375
- expert_down: bfloat16 [32, 1024, 4096], P('sp', None, 'tp'), may hold values from -0.1875 to 0.1875
- shared_gate: bfloat16 [4096, 1024], P(None, 'tp'), may hold values from -0.09375 to 0.09375
- shared_up: bfloat16 [4096, 1024], P(None, 'tp'), may hold values from -0.09375 to 0.09375
- shared_down: bfloat16 [1024, 4096], P(None, 'tp'), may hold values from -0.1875 to 0.1875
Outputs:
- mixed: bfloat16 [8192, 4096], P('sp', 'tp')
Inputs may be any that keep to these rules, and one draw needn't show every extreme that they name: `route_ids`: each row names 2 different experts. In each aligned block of 256 rows (the rows of one index of sp) no expert is named by more than 32 rows, a bound that some expert reaches in some blocks.
All inputs are finite; a program needn't handle non-finite values.
Results may differ from a plain program's by a relative error of at most 0.012.
Values may be sent and summed in bfloat16 or wider, within the bound.
A program may use at most 64 MiB of HBM per device.

v0:
```python
import jax
import jax.numpy as jnp
from jax import lax
from jax.sharding import PartitionSpec as P

D = 4096
CONV = 2048


norm_eps = 1e-06


def shifted(block, axis, distance):
    devices = range(lax.axis_size(axis))
    route = [(i - distance, i) for i in devices if i - distance in devices]
    return lax.ppermute(block, axis, route)


def from_everyone(array, axis):
    size = lax.axis_size(axis)
    return lax.all_to_all(
        jnp.broadcast_to(array[None], (size, *array.shape)), axis, 0, 0, tiled=True
    )


def over_copies(array, axis):
    return from_everyone(array, axis).sum(axis=0)


def in_one(arrays, axis):
    ravelled, at, gathered = (jnp.concatenate([a.reshape(-1) for a in arrays]), 0, [])
    subtotal = over_copies(ravelled, axis)
    for a in arrays:
        gathered.append(subtotal[at : at + a.size].reshape(a.shape))
        at += a.size
    return tuple(gathered)


def laid_out(pieces, dim):
    dims = list(pieces.shape[1:])
    dims[dim] *= pieces.shape[0]
    return jnp.moveaxis(pieces, 0, dim).reshape(dims)


def gather_directly(array, axis, dim):
    return laid_out(from_everyone(array, axis), dim)


def rows_first(arrays, axis, dims):
    turned = [jnp.moveaxis(a, dim, 0) for a, dim in zip(arrays, dims)]
    widths = [t[0].size for t in turned]
    both = jnp.concatenate([t.reshape(-1, w) for t, w in zip(turned, widths)], axis=1)
    out = lax.all_gather(both, axis, axis=0, tiled=True)
    pieces = jnp.split(out, [sum(widths[:k]) for k in range(1, len(widths))], axis=1)
    return tuple(
        (
            jnp.moveaxis(b.reshape(-1, *t.shape[1:]), 0, dim)
            for b, t, dim in zip(pieces, turned, dims)
        )
    )


def shards(
    u_val,
    u_gate,
    conv_weight,
    conv_bias,
    ln_gain,
    ln_bias,
    proj_weight,
    resid,
    norm_gain,
    route_ids,
    route_wts,
    expert_gate,
    expert_up,
    expert_down,
    shared_gate,
    shared_up,
    shared_down,
):
    tok_rows = u_val.shape[0]
    sp_count = lax.axis_size("sp")
    tp_count = lax.axis_size("tp")
    kernel_width = conv_weight.shape[0]
    gated = (u_val.astype(jnp.float32) * jax.nn.sigmoid(u_gate.astype(jnp.float32))).astype(
        jnp.bfloat16
    )
    rim_rows = shifted(gated[tok_rows - (kernel_width - 1) :], "sp", 1)
    padded = lax.optimization_barrier(jnp.concatenate([rim_rows, gated], axis=0)).astype(
        jnp.float32
    )
    conv_sum = jnp.zeros((tok_rows, gated.shape[1]), jnp.float32) + conv_bias[None, :]
    for tap_index in range(kernel_width):
        conv_sum = (
            conv_sum + conv_weight[tap_index][None, :] * padded[tap_index : tap_index + tok_rows]
        )
    stat_sums = in_one((jnp.sum(conv_sum, axis=1), jnp.sum(conv_sum * conv_sum, axis=1)), "tp")
    channel_mean = stat_sums[0] / CONV
    channel_var = stat_sums[1] / CONV - channel_mean * channel_mean
    normed_conv = (conv_sum - channel_mean[:, None]) * lax.rsqrt(channel_var + norm_eps)[:, None]
    conv_out = jax.nn.silu(normed_conv * ln_gain + ln_bias).astype(jnp.bfloat16)
    projected = jnp.dot(
        gather_directly(conv_out, "tp", 1), proj_weight, preferred_element_type=jnp.float32
    )
    residual_mid = (resid.astype(jnp.float32) + projected).astype(jnp.bfloat16)
    residual_wide = residual_mid.astype(jnp.float32)
    square_sum = over_copies(jnp.sum(residual_wide * residual_wide, axis=1), "tp")
    normed_rows = (
        residual_wide * lax.rsqrt(square_sum / D + norm_eps)[:, None] * norm_gain
    ).astype(jnp.bfloat16)
    rows_full = gather_directly(normed_rows, "tp", 1)
    topk_count = route_ids.shape[1]
    capacity = 2 * tok_rows * topk_count // sp_count
    pair_ids = route_ids.reshape(-1)
    onehot = (pair_ids[:, None] == jnp.arange(sp_count, dtype=jnp.int32)[None, :]).astype(jnp.int32)
    before = jnp.cumsum(onehot, axis=0) - onehot
    position = jnp.sum(before * onehot, axis=1)
    pair_slot = pair_ids * capacity + position
    matches = (
        jnp.arange(sp_count * capacity, dtype=jnp.int32)[:, None] == pair_slot[None, :]
    ).astype(jnp.int32)
    pair_tok = jnp.arange(tok_rows * topk_count, dtype=jnp.int32) // topk_count
    filled = jnp.sum(matches, axis=1)
    slot_tok = jnp.sum(matches * pair_tok[None, :], axis=1) + (1 - filled) * tok_rows
    rows_ext = jnp.concatenate(
        [rows_full, jnp.zeros((1, rows_full.shape[1]), jnp.bfloat16)], axis=0
    )
    part_slots = capacity // tp_count
    tp_index = lax.axis_index("tp")
    local_slots = lax.dynamic_slice_in_dim(
        slot_tok.reshape(sp_count, capacity), tp_index * part_slots, part_slots, 1
    )
    send_rows = jnp.take(rows_ext, local_slots.reshape(-1), axis=0).reshape(
        sp_count, part_slots, -1
    )
    received = lax.all_to_all(send_rows, "sp", split_axis=0, concat_axis=0, tiled=True)
    arrived = lax.all_gather(received, "tp", axis=1, tiled=True)
    slot_rows = arrived.reshape(sp_count * capacity, -1)
    gate_pre = jnp.dot(slot_rows, expert_gate[0], preferred_element_type=jnp.float32)
    up_proj = jnp.dot(slot_rows, expert_up[0], preferred_element_type=jnp.float32)
    hidden = (jax.nn.silu(gate_pre) * up_proj).astype(jnp.bfloat16)
    shared_pre = jnp.dot(rows_full, shared_gate, preferred_element_type=jnp.float32)
    shared_upper = jnp.dot(rows_full, shared_up, preferred_element_type=jnp.float32)
    shared_hidden = (jax.nn.silu(shared_pre) * shared_upper).astype(jnp.bfloat16)
    out_cols = expert_down.shape[2]
    pieces = rows_first((hidden, shared_hidden), "tp", (1, 1))
    routed_rows = expert_down[0]
    routed_out = jnp.dot(pieces[0], routed_rows, preferred_element_type=jnp.float32)
    shared_out = jnp.dot(pieces[1], shared_down, preferred_element_type=jnp.float32)
    expert_rows = routed_out.astype(jnp.bfloat16).reshape(sp_count, capacity, out_cols)
    returned_rows = lax.all_to_all(expert_rows, "sp", split_axis=0, concat_axis=0, tiled=True)
    returned_flat = returned_rows.reshape(sp_count * capacity, out_cols)
    picked = (
        jnp.take(returned_flat, pair_slot, axis=0)
        .astype(jnp.float32)
        .reshape(tok_rows, topk_count, out_cols)
    )
    routed = jnp.sum(picked * route_wts[:, :, None], axis=1)
    return (residual_wide + shared_out + routed).astype(jnp.bfloat16)


def solution(mesh):
    in_specs = (
        P("sp", "tp"),
        P("sp", "tp"),
        P(None, "tp"),
        P("tp"),
        P("tp"),
        P("tp"),
        P(None, "tp"),
        P("sp", "tp"),
        P("tp"),
        P("sp", None),
        P("sp", None),
        P("sp", None, "tp"),
        P("sp", None, "tp"),
        P("sp", None, "tp"),
        P(None, "tp"),
        P(None, "tp"),
        P(None, "tp"),
    )
    out_specs = P("sp", "tp")
    return jax.shard_map(shards, mesh=mesh, in_specs=in_specs, out_specs=out_specs, check_vma=False)
```

profile of v0, /device:TPU:1, one launch (start us, length us, event | category | flops | bytes accessed | tf_op | source)
XLA Modules:
  0.0 380.0 jit_solution(2414357554840305814)
XLA Ops:
  7.6 4.9 %collective-permute-start = (bf16[30,128]{1,0:T(8,128)(2,1)S(1)}, bf16[30,128]{1,0:T(8,128)(2,1)S(1)}, u32[]{:S(2)}, u32[]{:S(2)}) collective-permute-start(bf16[30,128]{1,0:T(8,128)(2,1)S(1)} %slice.272), channel_id=1, source_target_pairs={{0,16},{16,32},{32,48},{48,64},{64,80},{80,96},{96,112},{112,128},... | collective-permute-start | bytes 23048 | tf_op jit(solution)/shard_map/ppermute | solution.py:16
  14.5 1.9 collective-permute-done
  16.4 1.3 fusion.56
  17.7 11.3 %all_to_all.32 = f32[16,1,512]{2,1,0:T(1,128)S(1)} all-to-all(f32[16,1,512]{2,1,0:T(1,128)S(1)} %broadcast_in_dim.22), channel_id=1, replica_groups=mesh['sp'=32,'tp'=16] {'tp'}, dimensions={0} | all-to-all | bytes 65536 | tf_op jit(solution)/shard_map/all_to_all | solution.py:21
  29.4 1.1 broadcast_in_dim.23
  30.5 3.8 all-to-all-start.1
  34.4 16.9 %all-to-all-done.1 = bf16[16,256,128]{1,2,0:T(8,128)(2,1)S(1)} async-done(((bf16[16,256,128]{1,2,0:T(8,128)(2,1)}), bf16[16,256,128]{1,2,0:T(8,128)(2,1)S(1)}, u32[]{:S(2)}, u32[]{:S(2)}) %all-to-all-start.1) | async-done | bytes 1048608 | tf_op jit(solution)/shard_map/all_to_all | solution.py:21
  51.9 10.3 %all_to_all.33 = f32[16,1,256]{2,1,0:T(1,128)S(1)} all-to-all(f32[16,1,256]{2,1,0:T(1,128)S(1)} %broadcast_in_dim.25), channel_id=1, replica_groups=mesh['sp'=32,'tp'=16] {'tp'}, dimensions={0} | all-to-all | bytes 32768 | tf_op jit(solution)/shard_map/all_to_all | solution.py:21
  62.4 1.6 broadcast_in_dim.26
  64.0 3.8 %all-to-all-start.3 = ((bf16[16,256,256]{2,1,0:T(8,128)(2,1)}), bf16[16,256,256]{2,1,0:T(8,128)(2,1)S(1)}, u32[]{:S(2)}, u32[]{:S(2)}) async-start(bf16[16,256,256]{2,1,0:T(8,128)(2,1)} %broadcast_in_dim.26), calls=%async_computation.3 | async-start | bytes 4194304 | tf_op jit(solution)/shard_map/all_to_all | solution.py:21
  68.3 1.2 reduce-window.6
  70.8 24.7 %all-to-all-done.3 = bf16[16,256,256]{2,1,0:T(8,128)(2,1)S(1)} async-done(((bf16[16,256,256]{2,1,0:T(8,128)(2,1)}), bf16[16,256,256]{2,1,0:T(8,128)(2,1)S(1)}, u32[]{:S(2)}, u32[]{:S(2)}) %all-to-all-start.3) | async-done | bytes 2097184 | tf_op jit(solution)/shard_map/all_to_all | solution.py:21
  95.5 1.3 copy-done.2
  96.8 1.8 copy.131
  98.7 1.6 concatenate.14
  100.2 4.1 %gather_fusion = bf16[64,4096]{1,0:T(8,128)(2,1)} fusion(bf16[257,4096]{1,0:T(8,128)(2,1)} %concatenate.14, s32[1024]{0:T(1024)S(1)} %pad_clamp_fusion.1), kind=kCustom, calls=%fused_computation | custom fusion | bytes 1048832 | tf_op jit(solution)/shard_map/jit(_take)/gather | solution.py:134
  104.3 2.2 gather.13
  106.4 1.6 broadcast_select_fusion
  108.1 52.7 %all_to_all.34 = bf16[32,2,4096]{2,1,0:T(2,128)(2,1)S(1)} all-to-all(bf16[32,2,4096]{2,1,0:T(2,128)(2,1)S(1)} %broadcast_select_fusion), channel_id=1, replica_groups=mesh['sp'=32,'tp'=16] {'sp'}, dimensions={0} | all-to-all | bytes 1048576 | tf_op jit(solution)/shard_map/all_to_all | solution.py:137
  160.8 1.1 copy.116
  162.2 1.9 convolution_bitcast_fusion.3
  164.8 70.4 %all-gather.3.cloned.1.call-done = bf16[32,32,4096]{2,0,1:T(8,128)(2,1)} async-done(((bf16[32,2,4096]{2,0,1:T(8,128)(2,1)}), bf16[32,32,4096]{2,0,1:T(8,128)(2,1)}) %all-gather.3.cloned.1.call-update) | async-done | bytes 8388624 | tf_op jit(solution)/shard_map/all_gather | solution.py:138
  235.3 11.2 %copy.117 = bf16[32,32,4096]{2,1,0:T(8,128)(2,1)} copy(bf16[32,32,4096]{2,0,1:T(8,128)(2,1)} %all-gather.3.cloned.1.call-done) | data formatting | bytes 16777216 | tf_op jit(solution)/shard_map/all_gather | solution.py:138
  246.5 6.2 %convolution_bitcast_fusion.1 = f32[64,1024]{1,0:T(8,128)S(1)} fusion(bf16[1024,4096]{1,0:T(8,128)(2,1)} %bitcast.128, bf16[1,4096,64]{1,2,0:T(8,128)(2,1)S(1)} %copy-done.3), kind=kOutput, calls=%fused_computation.9 | convolution fusion | flops 536870912 | bytes 9175040 | tf_op jit(solution)/shard_map/dot_general | solution.py:140
  252.7 2.7 fusion.9
  256.1 60.2 %all-gather.5.cloned.1.call-done = bf16[1024,1280]{1,0:T(8,128)(2,1)} async-done(((bf16[64,1280]{1,0:T(8,128)(2,1)}), bf16[1024,1280]{1,0:T(8,128)(2,1)}) %all-gather.5.cloned.1.call-update) | async-done | bytes 2621456 | tf_op jit(solution)/shard_map/all_gather | solution.py:53
  316.3 3.2 fusion.2
  319.5 14.3 %all-to-all-start.5 = ((bf16[32,32,256]{2,1,0:T(8,128)(2,1)}), bf16[32,32,256]{2,1,0:T(8,128)(2,1)S(1)}, u32[]{:S(2)}, u32[]{:S(2)}) async-start(bf16[32,32,256]{2,1,0:T(8,128)(2,1)} %bitcast.44), calls=%async_computation.5 | async-start | bytes 1048576 | tf_op jit(solution)/shard_map/all_to_all | solution.py:152
  334.7 32.6 %all-to-all-done.5 = bf16[32,32,256]{2,1,0:T(8,128)(2,1)S(1)} async-done(((bf16[32,32,256]{2,1,0:T(8,128)(2,1)}), bf16[32,32,256]{2,1,0:T(8,128)(2,1)S(1)}, u32[]{:S(2)}, u32[]{:S(2)}) %all-to-all-start.5) | async-done | bytes 524320 | tf_op jit(solution)/shard_map/all_to_all | solution.py:152
  367.3 1.9 gather_fusion.1
  369.4 1.5 multiply_reduce_fusion
  371.0 1.4 fusion.10
  (81 shorter events, 9.6 us)
Async XLA Ops:
  6.5 44.8 %copy-start = (bf16[2048,256]{1,0:T(8,128)(2,1)S(1)}, bf16[2048,256]{1,0:T(8,128)(2,1)}, u32[]{:S(2)}) copy-start(bf16[2048,256]{1,0:T(8,128)(2,1)} %param.23) | copy-start | bytes 3145732
  7.6 8.8 %collective-permute-start = (bf16[30,128]{1,0:T(8,128)(2,1)S(1)}, bf16[30,128]{1,0:T(8,128)(2,1)S(1)}, u32[]{:S(2)}, u32[]{:S(2)}) collective-permute-start(bf16[30,128]{1,0:T(8,128)(2,1)S(1)} %slice.272), channel_id=1, source_target_pairs={{0,16},{16,32},{32,48},{48,64},{64,80},{80,96},{96,112},{112,128},... | collective-permute-start | bytes 23048 | tf_op jit(solution)/shard_map/ppermute | solution.py:16
  16.4 12.7 %copy-start.10 = (f32[128]{0:T(128)S(1)}, f32[128]{0:T(128)}, u32[]{:S(2)}) copy-start(f32[128]{0:T(128)} %param.22) | copy-start | bytes 1540
  16.4 12.7 %copy-start.11 = (f32[128]{0:T(128)S(1)}, f32[128]{0:T(128)}, u32[]{:S(2)}) copy-start(f32[128]{0:T(128)} %param.21) | copy-start | bytes 1540
  17.7 16.6 %copy-start.6 = (bf16[256,256]{1,0:T(8,128)(2,1)S(1)}, bf16[256,256]{1,0:T(8,128)(2,1)}, u32[]{:S(2)}) copy-start(bf16[256,256]{1,0:T(8,128)(2,1)} %param.24) | copy-start | bytes 393220
  30.5 31.7 %copy-start.9 = (f32[256]{0:T(256)S(1)}, f32[256]{0:T(256)}, u32[]{:S(2)}) copy-start(f32[256]{0:T(256)} %param.25) | copy-start | bytes 3076
  30.5 20.8 %all-to-all-start.1 = ((bf16[16,256,128]{1,2,0:T(8,128)(2,1)}), bf16[16,256,128]{1,2,0:T(8,128)(2,1)S(1)}, u32[]{:S(2)}, u32[]{:S(2)}) async-start(bf16[16,256,128]{1,2,0:T(8,128)(2,1)} %broadcast_in_dim.23), calls=%async_computation.1 | async-start | bytes 2097152 | tf_op jit(solution)/shard_map/all_to_all | solution.py:21
  64.0 3.9 %copy-start.7 = (s32[256,2]{0,1:T(2,128)S(1)}, s32[256,2]{0,1:T(2,128)}, u32[]{:S(2)}) copy-start(s32[256,2]{0,1:T(2,128)} %param.26) | copy-start | bytes 6148
  64.0 31.5 %all-to-all-start.3 = ((bf16[16,256,256]{2,1,0:T(8,128)(2,1)}), bf16[16,256,256]{2,1,0:T(8,128)(2,1)S(1)}, u32[]{:S(2)}, u32[]{:S(2)}) async-start(bf16[16,256,256]{2,1,0:T(8,128)(2,1)} %broadcast_in_dim.26), calls=%async_computation.3 | async-start | bytes 4194304 | tf_op jit(solution)/shard_map/all_to_all | solution.py:21
  67.8 167.5 %all-gather.3.cloned.1.call-start = ((), (), s32[]{:S(2)}) async-start(), calls=%async_computation.6 | async-start | bytes 8912896 | tf_op jit(solution)/shard_map/all_gather | solution.py:138
  95.5 1.4 copy-start.2
  162.0 154.3 %all-gather.5.cloned.1.call-start = ((), (), s32[]{:S(2)}) async-start(), calls=%async_computation.7 | async-start | bytes 2785280 | tf_op jit(solution)/shard_map/all_gather | solution.py:53
  162.2 1.9 copy-start.5
  164.8 81.6 %copy-start.3 = (bf16[1,4096,64]{1,2,0:T(8,128)(2,1)S(1)}, bf16[1,4096,64]{1,2,0:T(8,128)(2,1)}, u32[]{:S(2)}) copy-start(bf16[1,4096,64]{1,2,0:T(8,128)(2,1)} %param.28) | copy-start | bytes 1572868
  246.5 6.2 %copy-start.1 = (bf16[32,32,4096]{2,1,0:T(8,128)(2,1)S(1)}, bf16[32,32,4096]{2,1,0:T(8,128)(2,1)}, u32[]{:S(2)}) copy-start(bf16[32,32,4096]{2,1,0:T(8,128)(2,1)} %copy.117) | copy-start | bytes 25165828
  246.5 6.2 %copy-start.12 = (bf16[1,4096,64]{1,2,0:T(8,128)(2,1)S(1)}, bf16[1,4096,64]{1,2,0:T(8,128)(2,1)}, u32[]{:S(2)}) copy-start(bf16[1,4096,64]{1,2,0:T(8,128)(2,1)} %param.29) | copy-start | bytes 1572868
  252.7 63.6 %copy-start.13 = (bf16[1,1024,256]{2,1,0:T(8,128)(2,1)S(1)}, bf16[1,1024,256]{2,1,0:T(8,128)(2,1)}, u32[]{:S(2)}) copy-start(bf16[1,1024,256]{2,1,0:T(8,128)(2,1)} %param.30) | copy-start | bytes 1572868
  256.0 78.5 %copy-start.8 = (f32[256,2]{0,1:T(2,128)S(1)}, f32[256,2]{0,1:T(2,128)}, u32[]{:S(2)}) copy-start(f32[256,2]{0,1:T(2,128)} %param.27) | copy-start | bytes 6148
  319.5 47.8 %all-to-all-start.5 = ((bf16[32,32,256]{2,1,0:T(8,128)(2,1)}), bf16[32,32,256]{2,1,0:T(8,128)(2,1)S(1)}, u32[]{:S(2)}, u32[]{:S(2)}) async-start(bf16[32,32,256]{2,1,0:T(8,128)(2,1)} %bitcast.44), calls=%async_computation.5 | async-start | bytes 1048576 | tf_op jit(solution)/shard_map/all_to_all | solution.py:152
  334.5 36.5 %copy-start.4 = (bf16[1024,256]{1,0:T(8,128)(2,1)S(1)}, bf16[1024,256]{1,0:T(8,128)(2,1)}, u32[]{:S(2)}) copy-start(bf16[1024,256]{1,0:T(8,128)(2,1)} %param.33) | copy-start | bytes 1572868
Sparse Core Ops, SparseCore 0:
  162.1 73.1 all-gather.2
  256.2 60.0 all-gather.4
where the time goes:
time: 381 us; the launch traced here: 380 us
  waiting for transfers between devices  207 us (54%)
  blocking collectives  74.3 us (20%)
  local copies, waits for them, and re-layouts  32.9 us (9%)
  starting transfers between devices  27.1 us (7%)
  matrix products  16.6 us (4%)
  between operations  13.8 us (4%)
  other arithmetic  8.53 us (2%)
    all_gather x1, waiting for transfers between devices, shards(): arrived = lax.all_gather(received, 'tp', axis=1, tiled=True)  70.4 us
    all_gather x1, waiting for transfers between devices, rows_first(): out = lax.all_gather(both, axis, axis=0, tiled=True)  60.2 us
    all_to_all x1, blocking collectives, shards(): lax.all_to_all(send_rows, 'sp', split_axis=0, concat_axis=0, tiled=True)  52.7 us
    all_to_all x2, waiting for transfers between devices, from_everyone(): lax.all_to_all(jnp.broadcast_to(array[None], (size, *array.shape)), axis,...  41.6 us
    all_to_all x1, waiting for transfers between devices, shards(): lax.all_to_all(expert_rows, 'sp', split_axis=0, concat_axis=0, tiled=True)  32.6 us
    all_to_all x2, blocking collectives, from_everyone(): lax.all_to_all(jnp.broadcast_to(array[None], (size, *array.shape)), axis,...  21.6 us
    all_to_all x1, starting transfers between devices, shards(): lax.all_to_all(expert_rows, 'sp', split_axis=0, concat_axis=0, tiled=True)  14.3 us
    all_gather x1, local copies, waits for them, and re-layouts, shards(): arrived = lax.all_gather(received, 'tp', axis=1, tiled=True)  11.2 us
  transfers between devices with their start and end apart: 6, of which 6 were waited for; matrix products, arithmetic and copies ran while one was open for 2% of the time, Pallas kernels for 0%

commit v1 on v0

v1 whole, which is shorter than its diff:
```python
import jax
import jax.numpy as jnp
from jax import lax
from jax.experimental import pallas as pl
from jax.experimental.pallas import tpu as pltpu
from jax.sharding import PartitionSpec as P

MESH = pl.DeviceIdType.MESH
F32 = jnp.float32
BF16 = jnp.bfloat16

SP, TP, SIDE = 32, 16, 4
ROWS, CH, FEAT = 256, 128, 256
CONV, D = 2048, 4096
TAPS = 31
CAP = 32
SLOTS = SP * CAP
EPS = 1e-6


class Copies:
    def __init__(self, send, recv):
        self.send, self.recv, self.used, self.open = send, recv, 0, []

    def __call__(self, src, dst, target):
        k = self.used
        self.used += 1
        copy = pltpu.make_async_remote_copy(
            src_ref=src,
            dst_ref=dst,
            send_sem=self.send.at[k],
            recv_sem=self.recv.at[k],
            device_id=target,
            device_id_type=MESH,
        )
        copy.start()
        self.open.append(copy)
        return copy

    def drain(self):
        for copy in self.open:
            copy.wait_send()
        self.open = []


def wrap(i):
    return lax.rem(i + SIDE, SIDE)


class RingHalf:
    def __init__(self, copies, buf, lo, rows, first, y, x):
        self.copies, self.buf, self.lo, self.rows = copies, buf, lo, rows
        self.c1, self.c2 = (x, y) if first == "x" else (y, x)
        self.first = first

    def index(self, c1, c2):
        return c2 * SIDE + c1 if self.first == "x" else c1 * SIDE + c2

    def send(self, d1, d2, part, axis, step):
        half = self.rows // 2
        lo, n = {0: (self.lo, self.rows), 1: (self.lo, half), 2: (self.lo + half, half)}[part]
        src = self.index(wrap(self.c1 + d1), wrap(self.c2 + d2))
        ref = self.buf.at[src, pl.ds(lo, n)]
        to = (
            self.index(wrap(self.c1 + step), self.c2)
            if axis == 1
            else self.index(self.c1, wrap(self.c2 + step))
        )
        return self.copies(ref, ref, {"tp": to})

    def arrived(self, copy):
        copy.wait_recv()

    def rounds(self):
        one, two = {}, {}
        one["r"] = self.send(0, 0, 0, 1, 1)
        one["l"] = self.send(0, 0, 0, 1, -1)
        two[0] = (self.send(0, 0, 0, 2, 1), self.send(0, 0, 0, 2, -1))
        yield
        one["r"].wait_recv()
        fr = self.send(-1, 0, 1, 1, 1)
        two[-1] = (self.send(-1, 0, 0, 2, 1), self.send(-1, 0, 0, 2, -1))
        one["l"].wait_recv()
        fl = self.send(1, 0, 2, 1, -1)
        two[1] = (self.send(1, 0, 0, 2, 1), self.send(1, 0, 0, 2, -1))
        last = {}
        last[0] = self.forward(two, 0)
        yield
        fr.wait_recv()
        fl.wait_recv()
        two[2] = (self.send(2, 0, 0, 2, 1), self.send(2, 0, 0, 2, -1))
        last[-1] = self.forward(two, -1)
        last[1] = self.forward(two, 1)
        yield
        last[2] = self.forward(two, 2)
        for d in (0, -1, 1):
            for copy in last[d]:
                copy.wait_recv()
        yield
        for copy in last[2]:
            copy.wait_recv()

    def forward(self, two, d):
        right, left = two[d]
        right.wait_recv()
        a = self.send(d, -1, 1, 2, 1)
        left.wait_recv()
        b = self.send(d, 1, 2, 2, -1)
        return a, b


def gather_plane(copies, buf, rows, y, x):
    halves = (
        RingHalf(copies, buf, 0, rows // 2, "x", y, x).rounds(),
        RingHalf(copies, buf, rows // 2, rows // 2, "y", y, x).rounds(),
    )
    for _ in range(5):
        for half in halves:
            next(half, None)
        yield


def run(steps):
    for _ in steps:
        pass


def to_peers(copies, src, dst, me):
    return [copies(src, dst, {"tp": lax.rem(me + k, TP)}) for k in range(1, TP)]


def lanes(columns):
    rows = columns[0].shape[0]
    lane = lax.broadcasted_iota(jnp.int32, (rows, 128), 1)
    both = jnp.zeros((rows, 128), F32)
    for k, column in enumerate(columns):
        both = jnp.where(lane == k, column, both)
    return both.T


def columns(rows):
    n = rows[0].shape[1]
    sub = lax.broadcasted_iota(jnp.int32, (128, n), 0)
    both = jnp.zeros((128, n), F32)
    for k, row in enumerate(rows):
        both = jnp.where(sub == k, row, both)
    return both.T


def silu(v):
    return v / (1.0 + jnp.exp(-v))


def dot(a, b):
    return jnp.dot(a, b, preferred_element_type=F32)


def dot_t(a, b):
    return lax.dot_general(a, b, (((1,), (1,)), ((), ())), preferred_element_type=F32)


def kernel(
    u_val, u_gate, conv_weight, conv_bias, ln_gain, ln_bias, proj, resid, norm_gain, ids, wts,
    e_gate, e_up, e_down, s_gate, s_up, s_down,
    out,
    v_val, v_gate, v_cw, v_cb, v_lg, v_lb, v_proj, v_resid, v_ng, v_ids, v_wts,
    egu, sgu, w_lo, w_hi, s_lo, s_hi,
    in_sem,
    pad, conv, halo_out, halo_in, stat_out, stat_in, co, rm, ssq_out, ssq_in, na,
    disp, comb_hi, comb_lo, sent, got, ra, hid, back_out, back,
    send_sem, recv_sem,
):
    s, t = lax.axis_index("sp"), lax.axis_index("tp")
    y, x = t // SIDE, lax.rem(t, SIDE)

    barrier = pltpu.get_barrier_semaphore()
    for k in range(1, TP):
        pl.semaphore_signal(barrier, inc=1, device_id={"tp": lax.rem(t + k, TP)}, device_id_type=MESH)
    for k in range(1, SP):
        pl.semaphore_signal(barrier, inc=1, device_id={"sp": lax.rem(s + k, SP)}, device_id_type=MESH)

    loads = {}
    pairs = [
        (u_val, v_val), (u_gate, v_gate), (conv_weight, v_cw), (conv_bias, v_cb), (ln_gain, v_lg),
        (ln_bias, v_lb), (ids, v_ids), (wts, v_wts), (resid, v_resid), (norm_gain, v_ng), (proj, v_proj),
        (s_gate, sgu.at[pl.ds(0, 64)]), (s_up, sgu.at[pl.ds(64, 64)]),
        (e_gate.at[0], egu.at[pl.ds(0, 64)]), (e_up.at[0], egu.at[pl.ds(64, 64)]),
    ]
    for k, (src, dst) in enumerate(pairs):
        copy = pltpu.make_async_copy(src, dst, in_sem.at[k])
        copy.start()
        loads[k] = copy
    downs = []
    for k in range(TP):
        for n, (src, dst, at) in enumerate(
            ((e_down.at[0], w_lo, 0), (e_down.at[0], w_hi, 64), (s_down, s_lo, 0), (s_down, s_hi, 64))
        ):
            copy = pltpu.make_async_copy(
                src.at[pl.ds(64 * k, 64)], dst.at[k, pl.ds(at, 64)], in_sem.at[15 + 4 * k + n]
            )
            copy.start()
            downs.append(copy)
    for k in range(TP):
        for ref, at in ((w_lo, 64), (w_hi, 0), (s_lo, 64), (s_hi, 0)):
            ref[k, pl.ds(at, 64), :] = jnp.zeros((64, FEAT), BF16)

    copies = Copies(send_sem, recv_sem)

    for k in (0, 1):
        loads[k].wait()
    gate = v_gate[...].astype(F32)
    gated = (v_val[...].astype(F32) / (1.0 + jnp.exp(-gate))).astype(BF16)
    pad[pl.ds(32, ROWS), :] = gated.astype(F32)
    halo_out[...] = gated[ROWS - 32 :]

    for k in (6, 7):
        loads[k].wait()
    id_rows = v_ids[...].astype(F32)
    id_row = jnp.concatenate([id_rows[0:1], id_rows[1:2]], axis=1)
    expert = lax.broadcasted_iota(jnp.int32, (SP, 2 * ROWS), 0).astype(F32)
    named = (expert == id_row).astype(F32)
    earlier = (
        lax.broadcasted_iota(jnp.int32, (2 * ROWS, 2 * ROWS), 0)
        < lax.broadcasted_iota(jnp.int32, (2 * ROWS, 2 * ROWS), 1)
    ).astype(F32).astype(BF16)
    place = jnp.sum(dot(named.astype(BF16), earlier) * named, axis=0, keepdims=True)
    slot = id_row * CAP + place
    slot_0, slot_1 = slot[:, :ROWS], slot[:, ROWS:]
    row = lax.broadcasted_iota(jnp.int32, (SLOTS, ROWS), 0).astype(F32)
    disp[...] = jnp.where((row == slot_0) | (row == slot_1), 1.0, 0.0).astype(BF16)
    cols = columns([slot_0, slot_1, v_wts[0:1, :], v_wts[1:2, :]])
    col = lax.broadcasted_iota(jnp.int32, (ROWS, SLOTS), 1).astype(F32)
    weight = jnp.where(col == cols[:, 0:1], cols[:, 2:3], 0.0) + jnp.where(
        col == cols[:, 1:2], cols[:, 3:4], 0.0
    )
    high = weight.astype(BF16)
    comb_hi[...] = high
    comb_lo[...] = (weight - high.astype(F32)).astype(BF16)

    pl.semaphore_wait(barrier, TP - 1 + SP - 1)

    halo = copies(halo_out, halo_in, {"sp": lax.rem(s + 1, SP)})
    for k in (2, 3, 4, 5):
        loads[k].wait()
    halo.wait_recv()
    pad[pl.ds(0, 32), :] = jnp.where(s == 0, 0.0, halo_in[...].astype(F32))
    for part in range(2):
        total = jnp.broadcast_to(v_cb[...].reshape(1, CH), (128, CH))
        for tap in range(TAPS):
            total = total + v_cw[tap : tap + 1, :] * pad[pl.ds(128 * part + 2 + tap, 128), :]
        conv[pl.ds(128 * part, 128), :] = total

    mine = conv[...]
    mean = jnp.sum(mine, axis=1, keepdims=True) * (1.0 / CH)
    off = mine - mean
    stat_out[...] = lanes([mean, jnp.sum(off * off, axis=1, keepdims=True)])[0:8]
    stats = to_peers(copies, stat_out, stat_in.at[t], t)
    stat_in[t] = stat_out[...]
    for copy in stats:
        copy.wait_recv()
    means = stat_in[:, 0, :]
    total_mean = jnp.sum(means, axis=0, keepdims=True) * (1.0 / TP)
    off = means - total_mean
    var = (
        jnp.sum(stat_in[:, 1, :], axis=0, keepdims=True) + CH * jnp.sum(off * off, axis=0, keepdims=True)
    ) * (1.0 / CONV)
    cols = columns([total_mean, lax.rsqrt(var + EPS)])
    normed = (mine - cols[:, 0:1]) * cols[:, 1:2]
    co[t] = silu(normed * v_lg[...].reshape(1, CH) + v_lb[...].reshape(1, CH)).astype(BF16)
    run(gather_plane(copies, co, ROWS, y, x))

    for k in (8, 9, 10):
        loads[k].wait()
    acc = v_resid[...].astype(F32)
    for k in range(TP // 2):
        acc = acc + dot(jnp.concatenate([co[2 * k], co[2 * k + 1]], axis=1), v_proj[pl.ds(256 * k, 256), :])
    mid = acc.astype(BF16)
    rm[...] = mid
    wide = mid.astype(F32)
    ssq_out[...] = lanes([jnp.sum(wide * wide, axis=1, keepdims=True)])[0:8]
    squares = to_peers(copies, ssq_out, ssq_in.at[t], t)
    ssq_in[t] = ssq_out[...]
    for copy in squares:
        copy.wait_recv()
    scale = lax.rsqrt(jnp.sum(ssq_in[:, 0, :], axis=0, keepdims=True) * (1.0 / D) + EPS)
    na[t] = (wide * columns([scale])[:, 0:1] * v_ng[...].reshape(1, FEAT)).astype(BF16)

    rows = dot(disp[...], na[t]).astype(BF16)
    sent[...] = rows.reshape(SP, CAP, FEAT)
    moves = []
    for k in range(1, SP):
        e = lax.rem(s + SP - k, SP)
        moves.append(copies(sent.at[e], got.at[k], {"sp": e}))
    got[0] = sent[s]
    run(gather_plane(copies, na, ROWS, y, x))
    for k in (11, 12, 13, 14):
        loads[k].wait()
    lane = lax.broadcasted_iota(jnp.int32, (128, 128), 1)
    acc = jnp.zeros((ROWS, 128), F32)
    for k in range(TP):
        acc = acc + dot_t(na[k], sgu[:, pl.ds(FEAT * k, FEAT)])
    h = silu(acc) * pltpu.roll(acc, 64, axis=1)
    hid[t, pl.ds(512, 128), :] = jnp.where(lane < 64, h[:128], pltpu.roll(h[128:], 64, axis=1)).astype(BF16)

    for copy in moves:
        copy.wait_recv()
    ra[t] = got[...].reshape(SLOTS, FEAT)
    run(gather_plane(copies, ra, SLOTS, y, x))
    for part in range(4):
        lo, hi = pl.ds(128 * part, 128), pl.ds(512 + 128 * part, 128)
        a = jnp.zeros((128, 128), F32)
        b = jnp.zeros((128, 128), F32)
        for k in range(TP):
            w = egu[:, pl.ds(FEAT * k, FEAT)]
            a = a + dot_t(ra[k, lo, :], w)
            b = b + dot_t(ra[k, hi, :], w)
        a = silu(a) * pltpu.roll(a, 64, axis=1)
        b = silu(b) * pltpu.roll(b, 64, axis=1)
        hid[t, lo, :] = jnp.where(lane < 64, a, pltpu.roll(b, 64, axis=1)).astype(BF16)
    run(gather_plane(copies, hid, 640, y, x))

    for copy in downs:
        copy.wait()
    for part in range(4):
        for ref, at in ((w_lo, 0), (w_hi, 16)):
            acc = jnp.zeros((128, FEAT), F32)
            for k in range(TP):
                acc = acc + dot(hid[k, pl.ds(128 * part, 128), :], ref[k])
            back_out[pl.ds(at + 4 * part, 4)] = acc.astype(BF16).reshape(4, CAP, FEAT)
    moves = []
    for k in range(1, SP):
        moves.append(copies(back_out.at[k], back.at[s], {"sp": lax.rem(s + k, SP)}))
    back[s] = back_out[0]
    acc = rm[...].astype(F32)
    for n, ref in enumerate((s_lo, s_hi)):
        part = jnp.zeros((128, FEAT), F32)
        for k in range(TP):
            part = part + dot(hid[k, pl.ds(512, 128), :], ref[k])
        if n == 0:
            first = part
    acc = acc + jnp.concatenate([first, part], axis=0)
    for copy in moves:
        copy.wait_recv()
    full = back[...].reshape(SLOTS, FEAT)
    acc = acc + dot(comb_hi[...], full) + dot(comb_lo[...], full)
    out[...] = acc.astype(BF16)
    copies.drain()


def shards(*args):
    args = list(args)
    for k in (9, 10, 14, 15):
        args[k] = args[k].T
    for k in (11, 12):
        args[k] = jnp.swapaxes(args[k], 1, 2)
    bf, f = (lambda *shape: pltpu.VMEM(shape, BF16)), (lambda *shape: pltpu.VMEM(shape, F32))
    n_copies = 1 + 15 + 40 + 15 + 31 + 40 + 40 + 40 + 31
    return pl.pallas_call(
        kernel,
        name="layer",
        out_shape=jax.ShapeDtypeStruct((ROWS, FEAT), BF16),
        in_specs=[pl.BlockSpec(memory_space=pltpu.HBM)] * 17,
        out_specs=pl.BlockSpec(memory_space=pltpu.VMEM),
        scratch_shapes=[
            bf(ROWS, CH), bf(ROWS, CH), f(TAPS, CH), f(CH), f(CH), f(CH), bf(CONV, FEAT), bf(ROWS, FEAT), f(FEAT),
            pltpu.VMEM((2, ROWS), jnp.int32), f(2, ROWS),
            bf(128, D), bf(128, D),
            bf(TP, 128, FEAT), bf(TP, 128, FEAT), bf(TP, 128, FEAT), bf(TP, 128, FEAT),
            pltpu.SemaphoreType.DMA((15 + 64,)),
            f(32 + ROWS, CH), f(ROWS, CH), bf(32, CH), bf(32, CH), f(8, ROWS), f(TP, 8, ROWS), bf(TP, ROWS, CH),
            bf(ROWS, FEAT), f(8, ROWS), f(TP, 8, ROWS), bf(TP, ROWS, FEAT),
            bf(SLOTS, ROWS), bf(ROWS, SLOTS), bf(ROWS, SLOTS),
            bf(SP, CAP, FEAT), bf(SP, CAP, FEAT), bf(TP, SLOTS, FEAT), bf(TP, 640, 128),
            bf(SP, CAP, FEAT), bf(SP, CAP, FEAT),
            pltpu.SemaphoreType.DMA((n_copies,)), pltpu.SemaphoreType.DMA((n_copies,)),
        ],
        compiler_params=pltpu.CompilerParams(
            collective_id=0, has_side_effects=True, vmem_limit_bytes=60 * 2**20
        ),
    )(*args)


def solution(mesh):
    in_specs = (
        P("sp", "tp"), P("sp", "tp"), P(None, "tp"), P("tp"), P("tp"), P("tp"), P(None, "tp"), P("sp", "tp"), P("tp"),
        P("sp", None), P("sp", None), P("sp", None, "tp"), P("sp", None, "tp"), P("sp", None, "tp"),
        P(None, "tp"), P(None, "tp"), P(None, "tp"),
    )
    return jax.shard_map(shards, mesh=mesh, in_specs=in_specs, out_specs=P("sp", "tp"), check_vma=False)
```

time: 381 us -> 169 us (0.44)
  waiting for transfers between devices: 207 us -> 0 us
  Pallas kernels: 0 us -> 168 us
  blocking collectives: 74.3 us -> 0 us
  local copies, waits for them, and re-layouts: 32.9 us -> 1.57 us
  starting transfers between devices: 27.1 us -> 0 us
  matrix products: 16.6 us -> 0 us
  between operations: 13.8 us -> 0.01 us
  other arithmetic: 8.53 us -> 0 us
    pallas_call x0 -> x1, Pallas kernels: none -> 168 us  [shards(): pl.pallas_call(kernel, name='layer', out_shape=jax.ShapeDtypeStruct((ROWS...]
    all_gather x2 -> x0, waiting for transfers between devices: 131 us -> none  [the longest x1 70.4 us: shards(): arrived = lax.all_gather(received, 'tp', axis=1, tiled=True)]
    all_to_all x3 -> x0, blocking collectives: 74.3 us -> none  [the longest x1 52.7 us: shards(): lax.all_to_all(send_rows, 'sp', split_axis=0, concat_axis=0, tiled=True)]
    all_to_all x3 -> x0, waiting for transfers between devices: 74.2 us -> none  [the longest x2 41.6 us: from_everyone(): lax.all_to_all(jnp.broadcast_to(array[None], (size, *array.shape)), axis,...]
    all_to_all x3 -> x0, starting transfers between devices: 22 us -> none  [the longest x1 14.3 us: shards(): lax.all_to_all(expert_rows, 'sp', split_axis=0, concat_axis=0, tiled=True)]
    dot_general x7 -> x0, matrix products: 16.6 us -> none  [the longest x1 6.19 us: shards(): jnp.dot(slot_rows, expert_gate[0], preferred_element_type=jnp.float32)]
    all_gather x1 -> x0, local copies, waits for them, and re-layouts: 11.2 us -> none  [shards(): arrived = lax.all_gather(received, 'tp', axis=1, tiled=True)]
    gather x4 -> x0, local copies, waits for them, and re-layouts: 8.27 us -> none  [the longest x2 6.22 us: shards(): jnp.take(rows_ext, local_slots.reshape(-1), axis=0)]
  transfers between devices with their start and end apart: 6 -> 0, of which waited for: 6 -> 0; matrix products, arithmetic and copies ran while one was open for 2% -> 0% of each run, Pallas kernels for 0% -> 0%
where the time goes in v1:
time: 169 us
  Pallas kernels  168 us (99%)
    pallas_call x1, Pallas kernels, shards(): pl.pallas_call(kernel, name='layer', out_shape=jax.ShapeDtypeStruct((ROWS...  168 us

profile of v1, /device:TPU:1, one launch (start us, length us, event | category | flops | bytes accessed | tf_op | source)
XLA Modules:
  0.0 169.2 jit_solution(16620413705074064060)
XLA Ops:
  0.0 167.7 %layer.1 = bf16[256,256]{1,0:T(8,128)(2,1)} custom-call(bf16[256,128]{1,0:T(8,128)(2,1)} %u_val.1, bf16[256,128]{1,0:T(8,128)(2,1)} %u_gate.1, f32[31,128]{1,0:T(8,128)} %conv_weight.1, f32[128]{0:T(128)} %conv_bias.1, f32[128]{0:T(128)} %ln_gain.1, f32[128]{0:T(128)} %ln_bias.1, bf16[2048,256]{1,0:T(8,128)(2,1)} %proj.1, bf16[256,256]{1,0:T(8,128)(2,1)} %resid.1, ...), custom_call_target="tpu_custom_call" | custom-call | tf_op jit(solution)/shard_map/layer/pallas_call | solution.py:358
  167.7 1.6 copy.19

commit v2 on v1

v2 whole, which is shorter than its diff:
```python
import heapq

import jax
import jax.numpy as jnp
from jax import lax
from jax.experimental import pallas as pl
from jax.experimental.pallas import tpu as pltpu
from jax.sharding import PartitionSpec as P

MESH = pl.DeviceIdType.MESH
F32 = jnp.float32
BF16 = jnp.bfloat16

SP, TP, SIDE = 32, 16, 4
ROWS, CH, FEAT = 256, 128, 256
CONV, D = 2048, 4096
TAPS = 31
CAP = 32
SLOTS = SP * CAP
CHUNKS = 4
SENDS, RECVS = 9 + 3 * CHUNKS, 5 + 24 * 3 + CHUNKS * (1 + 3 + 1 + 24)
ORDER = (3, 4, 2, 5, 1, 6, 0, 7)
EPS = 1e-6


def arrived(ref, sem):
    pltpu.make_async_copy(ref, ref, sem).wait()


class Copies:
    def __init__(self, send, recv):
        self.send, self.recv, self.sends, self.recvs, self.open = send, recv, 0, 0, []

    def group(self, ref):
        sem = self.send.at[self.sends]
        self.sends += 1
        self.open.append((ref, sem))
        return sem

    def landing(self):
        self.recvs += 1
        return self.recv.at[self.recvs - 1]

    def __call__(self, src, dst, target, send, recv):
        pltpu.make_async_remote_copy(
            src_ref=src, dst_ref=dst, send_sem=send, recv_sem=recv, device_id=target, device_id_type=MESH
        ).start()

    def drain(self):
        for ref, sem in self.open:
            arrived(ref, sem)


def wrap(i):
    return lax.rem(i + SIDE, SIDE)


class RingHalf:
    def __init__(self, copies, out, buf, lo, rows, first, y, x):
        self.copies, self.out, self.buf, self.lo, self.rows = copies, out, buf, lo, rows
        self.c1, self.c2 = (x, y) if first == "x" else (y, x)
        self.first = first

    def index(self, c1, c2):
        return c2 * SIDE + c1 if self.first == "x" else c1 * SIDE + c2

    def send(self, d1, d2, part, axis, step, sem=None):
        half = self.rows // 2
        lo, n = {0: (self.lo, self.rows), 1: (self.lo, half), 2: (self.lo + half, half)}[part]
        src = self.index(wrap(self.c1 + d1), wrap(self.c2 + d2))
        ref = self.buf.at[src, pl.ds(lo, n)]
        to = (
            self.index(wrap(self.c1 + step), self.c2)
            if axis == 1
            else self.index(self.c1, wrap(self.c2 + step))
        )
        sem = self.copies.landing() if sem is None else sem
        self.copies(ref, ref, {"tp": to}, self.out, sem)
        return sem

    def block(self, sem):
        arrived(self.buf.at[0, pl.ds(0, self.rows)], sem)

    def both(self, d):
        return self.send(d, 0, 0, 2, 1), self.send(d, 0, 0, 2, -1)

    def rounds(self):
        right = self.send(0, 0, 0, 1, 1)
        left = self.send(0, 0, 0, 1, -1)
        two = {0: self.both(0)}
        yield
        self.block(right)
        far = self.send(-1, 0, 1, 1, 1)
        two[-1] = self.both(-1)
        self.block(left)
        self.send(1, 0, 2, 1, -1, far)
        two[1] = self.both(1)
        last = self.copies.landing()
        self.forward(two, 0, last)
        yield
        self.block(far)
        two[2] = self.both(2)
        self.forward(two, -1, last)
        self.forward(two, 1, last)
        yield
        self.forward(two, 2, last)
        yield
        arrived(self.buf.at[pl.ds(0, 2)], last)

    def forward(self, two, d, last):
        right, left = two[d]
        self.block(right)
        self.send(d, -1, 1, 2, 1, last)
        self.block(left)
        self.send(d, 1, 2, 2, -1, last)


def gather_plane(copies, buf, rows, y, x):
    out = copies.group(buf.at[pl.ds(0, TP - 1)])
    halves = (
        RingHalf(copies, out, buf, 0, rows // 2, "x", y, x).rounds(),
        RingHalf(copies, out, buf, rows // 2, rows // 2, "y", y, x).rounds(),
    )
    for _ in range(5):
        for half in halves:
            next(half, None)
        yield


def run(steps):
    for _ in steps:
        pass


def ready(loads):
    while loads:
        arrived(*loads.pop())


def interleave(tasks):
    queue = [(at, n, task) for n, (at, task) in enumerate(tasks)]
    heapq.heapify(queue)
    while queue:
        now, n, task = heapq.heappop(queue)
        later = next(task, None)
        if later is not None:
            heapq.heappush(queue, (now + later, n, task))


def to_peers(copies, src, dst, me):
    out, sem = copies.group(dst.at[pl.ds(0, TP - 1)]), copies.landing()
    for k in range(1, TP):
        copies(src, dst.at[me], {"tp": lax.rem(me + k, TP)}, out, sem)
    return sem


def lanes(columns):
    rows = columns[0].shape[0]
    lane = lax.broadcasted_iota(jnp.int32, (rows, 128), 1)
    both = jnp.zeros((rows, 128), F32)
    for k, column in enumerate(columns):
        both = jnp.where(lane == k, column, both)
    return both.T


def columns(rows):
    n = rows[0].shape[1]
    sub = lax.broadcasted_iota(jnp.int32, (128, n), 0)
    both = jnp.zeros((128, n), F32)
    for k, row in enumerate(rows):
        both = jnp.where(sub == k, row, both)
    return both.T


def silu(v):
    return v / (1.0 + jnp.exp(-v))


def dot(a, b):
    return jnp.dot(a, b, preferred_element_type=F32)


def dot_t(a, b):
    return lax.dot_general(a, b, (((1,), (1,)), ((), ())), preferred_element_type=F32)


class Phases:
    def __init__(self):
        self.scope = None

    def __call__(self, name):
        if self.scope is not None:
            self.scope.__exit__(None, None, None)
        self.scope = jax.named_scope(name) if name else None
        if name:
            self.scope.__enter__()


def kernel(
    u_val, u_gate, conv_weight, conv_bias, ln_gain, ln_bias, proj, resid, norm_gain, ids, wts,
    e_gate, e_up, e_down, s_gate, s_up, s_down,
    out,
    v_val, v_gate, v_cw, v_cb, v_lg, v_lb, v_proj, v_resid, v_ng, v_ids, v_wts,
    ewt, w2, sgu, w_lo, w_hi, s_lo, s_hi,
    in_sem,
    pad, conv, halo_out, halo_in, stat_out, stat_in, co, rm, ssq_out, ssq_in, na,
    disp, comb_hi, comb_lo, sent, ya, rs_out, rs_in, hid, shared_out, back_out, back,
    send_sem, recv_sem,
):
    s, t = lax.axis_index("sp"), lax.axis_index("tp")
    y, x = t // SIDE, lax.rem(t, SIDE)

    phase = Phases()
    phase("start")
    barrier = pltpu.get_barrier_semaphore()
    for k in range(1, TP):
        pl.semaphore_signal(barrier, inc=1, device_id={"tp": lax.rem(t + k, TP)}, device_id_type=MESH)
    for k in range(1, SP):
        pl.semaphore_signal(barrier, inc=1, device_id={"sp": lax.rem(s + k, SP)}, device_id_type=MESH)

    loads = {}
    pairs = [
        (u_val, v_val), (u_gate, v_gate), (conv_weight, v_cw), (conv_bias, v_cb), (ln_gain, v_lg),
        (ln_bias, v_lb), (ids, v_ids), (wts, v_wts), (resid, v_resid), (norm_gain, v_ng), (proj, v_proj),
        (s_gate, sgu.at[pl.ds(0, 64)]), (s_up, sgu.at[pl.ds(64, 64)]),
    ]
    for k, (src, dst) in enumerate(pairs):
        copy = pltpu.make_async_copy(src, dst, in_sem.at[k])
        copy.start()
        loads[k] = copy
    for k in range(TP):
        for n, (src, dst, at) in enumerate(
            ((e_down.at[0], w_lo, 0), (e_down.at[0], w_hi, 64), (s_down, s_lo, 0), (s_down, s_hi, 64))
        ):
            pltpu.make_async_copy(
                src.at[pl.ds(64 * k, 64)], dst.at[k, pl.ds(at, 64)], in_sem.at[13 + n]
            ).start()
    downs = [(ref.at[pl.ds(0, TP // 2)], in_sem.at[13 + n]) for n, ref in enumerate((w_lo, w_hi, s_lo, s_hi))]
    for k in range(TP):
        for n, src in enumerate((e_gate, e_up)):
            pltpu.make_async_copy(
                src.at[0, :, pl.ds(FEAT * k, FEAT)], ewt.at[k, pl.ds(64 * n, 64)], in_sem.at[17]
            ).start()
    for k in range(TP):
        for ref, at in ((w_lo, 64), (w_hi, 0), (s_lo, 64), (s_hi, 0)):
            ref[k, pl.ds(at, 64), :] = jnp.zeros((64, FEAT), BF16)

    copies = Copies(send_sem, recv_sem)

    spread_out, spread_in = copies.group(w2.at[pl.ds(0, 3)]), copies.landing()

    def spread(k):
        for n in (2, 1, 3):
            to = wrap(x + n)
            copies(ewt.at[SIDE * k + to], w2.at[k, x], {"tp": y * SIDE + to}, spread_out, spread_in)

    phase("gated")
    for k in (0, 1):
        loads[k].wait()
    gate = v_gate[...].astype(F32)
    gated = (v_val[...].astype(F32) / (1.0 + jnp.exp(-gate))).astype(BF16)
    pad[pl.ds(32, ROWS), :] = gated.astype(F32)
    halo_out[...] = gated[ROWS - 32 :]

    phase("slots")
    for k in (6, 7):
        loads[k].wait()
    id_rows = v_ids[...].astype(F32)
    id_row = jnp.concatenate([id_rows[0:1], id_rows[1:2]], axis=1)
    expert = lax.broadcasted_iota(jnp.int32, (SP, 2 * ROWS), 0).astype(F32)
    named = (expert == id_row).astype(F32)
    earlier = (
        lax.broadcasted_iota(jnp.int32, (2 * ROWS, 2 * ROWS), 0)
        < lax.broadcasted_iota(jnp.int32, (2 * ROWS, 2 * ROWS), 1)
    ).astype(F32).astype(BF16)
    place = jnp.sum(dot(named.astype(BF16), earlier) * named, axis=0, keepdims=True)
    slot = id_row * CAP + place
    slot_0, slot_1 = slot[:, :ROWS], slot[:, ROWS:]
    row = lax.broadcasted_iota(jnp.int32, (SLOTS, ROWS), 0).astype(F32)
    disp[...] = jnp.where((row == slot_0) | (row == slot_1), 1.0, 0.0).astype(BF16)
    cols = columns([slot_0, slot_1, v_wts[0:1, :], v_wts[1:2, :]])
    col = lax.broadcasted_iota(jnp.int32, (ROWS, SLOTS), 1).astype(F32)
    weight = jnp.where(col == cols[:, 0:1], cols[:, 2:3], 0.0) + jnp.where(
        col == cols[:, 1:2], cols[:, 3:4], 0.0
    )
    high = weight.astype(BF16)
    comb_hi[...] = high
    comb_lo[...] = (weight - high.astype(F32)).astype(BF16)

    phase("barrier")
    pl.semaphore_wait(barrier, TP - 1 + SP - 1)

    phase("halo")
    halo = copies.landing()
    copies(halo_out, halo_in, {"sp": lax.rem(s + 1, SP)}, copies.group(halo_in), halo)
    for k in (2, 3, 4, 5):
        loads[k].wait()
    arrived(halo_in, halo)
    pad[pl.ds(0, 32), :] = jnp.where(s == 0, 0.0, halo_in[...].astype(F32))
    phase("conv")
    for part in range(2):
        total = jnp.broadcast_to(v_cb[...].reshape(1, CH), (128, CH))
        for tap in range(TAPS):
            total = total + v_cw[tap : tap + 1, :] * pad[pl.ds(128 * part + 2 + tap, 128), :]
        conv[pl.ds(128 * part, 128), :] = total

    phase("stats")
    mine = conv[...]
    mean = jnp.sum(mine, axis=1, keepdims=True) * (1.0 / CH)
    off = mine - mean
    stat_out[...] = lanes([mean, jnp.sum(off * off, axis=1, keepdims=True)])[0:8]
    stats = to_peers(copies, stat_out, stat_in, t)
    arrived(ewt, in_sem.at[17])
    spread(0)
    for k in range(SIDE):
        w2[k, x] = ewt[SIDE * k + x]
    stat_in[t] = stat_out[...]
    arrived(stat_in.at[pl.ds(0, TP - 1)], stats)
    means = stat_in[:, 0, :]
    total_mean = jnp.sum(means, axis=0, keepdims=True) * (1.0 / TP)
    off = means - total_mean
    var = (
        jnp.sum(stat_in[:, 1, :], axis=0, keepdims=True) + CH * jnp.sum(off * off, axis=0, keepdims=True)
    ) * (1.0 / CONV)
    cols = columns([total_mean, lax.rsqrt(var + EPS)])
    normed = (mine - cols[:, 0:1]) * cols[:, 1:2]
    co[t] = silu(normed * v_lg[...].reshape(1, CH) + v_lb[...].reshape(1, CH)).astype(BF16)
    phase("gather_co")
    run(gather_plane(copies, co, ROWS, y, x))

    phase("project")
    for k in (8, 9, 10):
        loads[k].wait()
    acc = v_resid[...].astype(F32)
    for k in range(TP // 2):
        acc = acc + dot(jnp.concatenate([co[2 * k], co[2 * k + 1]], axis=1), v_proj[pl.ds(256 * k, 256), :])
    mid = acc.astype(BF16)
    rm[...] = mid
    wide = mid.astype(F32)
    ssq_out[...] = lanes([jnp.sum(wide * wide, axis=1, keepdims=True)])[0:8]
    phase("ssq")
    squares = to_peers(copies, ssq_out, ssq_in, t)
    spread(1)
    ssq_in[t] = ssq_out[...]
    arrived(ssq_in.at[pl.ds(0, TP - 1)], squares)
    scale = lax.rsqrt(jnp.sum(ssq_in[:, 0, :], axis=0, keepdims=True) * (1.0 / D) + EPS)
    na[t] = (wide * columns([scale])[:, 0:1] * v_ng[...].reshape(1, FEAT)).astype(BF16)

    phase("dispatch")
    rows = dot(disp[...], na[t]).astype(BF16)
    sent[...] = rows.reshape(SP, CAP, FEAT)
    moves_out = copies.group(sent.at[pl.ds(0, SP - 1)])
    moves = [copies.landing() for c in range(CHUNKS)]

    def dispatch(c):
        phase(f"send{c}")
        for j in ORDER:
            k = CHUNKS * j + c
            if k:
                e = lax.rem(s + SP - k, SP)
                copies(sent.at[e], ya.at[c, y, pl.ds(CAP * j, CAP)], {"sp": e}, moves_out, moves[c])
        yield None

    ya[0, y, pl.ds(0, CAP), :] = sent[s]
    lane = lax.broadcasted_iota(jnp.int32, (128, 128), 1)

    def hidden(acc):
        h = silu(acc) * pltpu.roll(acc, 64, axis=1)
        return jnp.where(lane < 64, h[:128], pltpu.roll(h[128:], 64, axis=1)).astype(BF16)

    def down(c, lo, hi):
        both = []
        for ref in (lo, hi):
            acc = jnp.zeros((128, FEAT), F32)
            for k in range(TP // 2):
                pair = jnp.concatenate([hid[c, 2 * k], hid[c, 2 * k + 1]], axis=1)
                acc = acc + dot(pair, ref[pl.ds(2 * k, 2)].reshape(2 * 128, FEAT))
            both.append(acc)
        return both

    def more():
        for k in range(2, 4):
            spread(k)
        yield None

    def shared():
        phase("shared")
        for _ in gather_plane(copies, na, ROWS, y, x):
            yield 3.0
        for k in (11, 12):
            loads[k].wait()
        acc = jnp.zeros((ROWS, 128), F32)
        for k in range(TP):
            acc = acc + dot_t(na[k], sgu[:, pl.ds(FEAT * k, FEAT)])
        hid[CHUNKS, t] = hidden(acc)
        for _ in gather_plane(copies, hid.at[CHUNKS], 128, y, x):
            yield 4.0
        ready(downs)
        lo, hi = down(CHUNKS, s_lo, s_hi)
        shared_out[pl.ds(0, 128), :] = lo
        shared_out[pl.ds(128, 128), :] = hi

    returns_out, returns = copies.group(back.at[pl.ds(0, SP - 1)]), copies.landing()

    def routed(c):
        phase(f"arrive{c}")
        arrived(ya.at[c, 0, pl.ds(0 if c else CAP, ROWS if c else ROWS - CAP)], moves[c])
        out = copies.group(ya.at[c, pl.ds(0, 3)])
        a, b, far = copies.landing(), copies.landing(), copies.landing()
        up_y, down_y = {"tp": wrap(y + 1) * SIDE + x}, {"tp": wrap(y - 1) * SIDE + x}
        copies(ya.at[c, y], ya.at[c, y], up_y, out, a)
        copies(ya.at[c, y], ya.at[c, y], down_y, out, b)
        yield 4.5
        phase(f"ya{c}")
        arrived(ya.at[c, 0], a)
        at = ya.at[c, wrap(y - 1), pl.ds(0, 128)]
        copies(at, at, up_y, out, far)
        arrived(ya.at[c, 0], b)
        at = ya.at[c, wrap(y + 1), pl.ds(128, 128)]
        copies(at, at, down_y, out, far)
        yield 3.0
        phase(f"yb{c}")
        arrived(ya.at[c, 0], far)
        if c == 0:
            arrived(w2.at[pl.ds(0, 3)], spread_in)
        phase(f"up{c}")
        acc = jnp.zeros((ROWS, 4 * 128), F32)
        for k in range(SIDE):
            acc = acc + dot_t(ya[c, k], w2[k].reshape(4 * 128, FEAT))
        for k in range(SIDE):
            rs_out[c, k] = acc[:, 128 * k : 128 * (k + 1)].astype(BF16)
        out, parts = copies.group(rs_in.at[c, pl.ds(0, 3)]), copies.landing()
        for k in (2, 1, 3):
            to = wrap(x + k)
            copies(rs_out.at[c, to], rs_in.at[c, x], {"tp": y * SIDE + to}, out, parts)
        yield 5.0
        phase(f"rs{c}")
        arrived(rs_in.at[c, pl.ds(0, 3)], parts)
        acc = rs_out[c, x].astype(F32)
        for k in range(1, SIDE):
            acc = acc + rs_in[c, wrap(x + k)].astype(F32)
        hid[c, t] = hidden(acc)
        for n, _ in enumerate(gather_plane(copies, hid.at[c], 128, y, x)):
            yield 2.6
            phase(f"hid{c}{n}")
        ready(downs)
        phase(f"down{c}")
        lo, hi = down(c, w_lo, w_hi)
        back_out[c, pl.ds(0, 4)] = lo.astype(BF16).reshape(4, CAP, FEAT)
        back_out[c, pl.ds(4, 4)] = hi.astype(BF16).reshape(4, CAP, FEAT)
        for j in ORDER:
            k = CHUNKS * j + c
            if k:
                copies(back_out.at[c, j], back.at[s], {"sp": lax.rem(s + k, SP)}, returns_out, returns)

    tasks = [(4.5 * c, dispatch(c)) for c in range(CHUNKS)]
    tasks += [(0.0, more()), (0.1, shared())]
    tasks += [(10.0 + 4.5 * c, routed(c)) for c in range(CHUNKS)]
    interleave(tasks)
    back[s] = back_out[0, 0]
    phase("back_wait")
    arrived(back.at[pl.ds(0, SP - 1)], returns)
    phase("combine")
    full = back[...].reshape(SLOTS, FEAT)
    acc = rm[...].astype(F32) + shared_out[...] + dot(comb_hi[...], full) + dot(comb_lo[...], full)
    out[...] = acc.astype(BF16)
    phase("drain")
    copies.drain()
    assert (copies.sends, copies.recvs) == (SENDS, RECVS), (copies.sends, copies.recvs)
    phase(None)


def shards(*args):
    args = list(args)
    for k in (9, 10, 14, 15):
        args[k] = args[k].T
    for k in (11, 12):
        args[k] = jnp.swapaxes(args[k], 1, 2)
    bf, f = (lambda *shape: pltpu.VMEM(shape, BF16)), (lambda *shape: pltpu.VMEM(shape, F32))
    return pl.pallas_call(
        kernel,
        name="layer",
        out_shape=jax.ShapeDtypeStruct((ROWS, FEAT), BF16),
        in_specs=[pl.BlockSpec(memory_space=pltpu.HBM)] * 17,
        out_specs=pl.BlockSpec(memory_space=pltpu.VMEM),
        scratch_shapes=[
            bf(ROWS, CH), bf(ROWS, CH), f(TAPS, CH), f(CH), f(CH), f(CH), bf(CONV, FEAT), bf(ROWS, FEAT), f(FEAT),
            pltpu.VMEM((2, ROWS), jnp.int32), f(2, ROWS),
            bf(TP, 128, FEAT), bf(SIDE, SIDE, 128, FEAT), bf(128, D),
            bf(TP, 128, FEAT), bf(TP, 128, FEAT), bf(TP, 128, FEAT), bf(TP, 128, FEAT),
            pltpu.SemaphoreType.DMA((18,)),
            f(32 + ROWS, CH), f(ROWS, CH), bf(32, CH), bf(32, CH), f(8, ROWS), f(TP, 8, ROWS), bf(TP, ROWS, CH),
            bf(ROWS, FEAT), f(8, ROWS), f(TP, 8, ROWS), bf(TP, ROWS, FEAT),
            bf(SLOTS, ROWS), bf(ROWS, SLOTS), bf(ROWS, SLOTS),
            bf(SP, CAP, FEAT), bf(CHUNKS, SIDE, ROWS, FEAT), bf(CHUNKS, SIDE, ROWS, 128), bf(CHUNKS, SIDE, ROWS, 128),
            bf(CHUNKS + 1, TP, 128, 128), f(ROWS, FEAT), bf(CHUNKS, SP // CHUNKS, CAP, FEAT), bf(SP, CAP, FEAT),
            pltpu.SemaphoreType.DMA((SENDS,)), pltpu.SemaphoreType.DMA((RECVS,)),
        ],
        compiler_params=pltpu.CompilerParams(
            collective_id=0, has_side_effects=True, vmem_limit_bytes=60 * 2**20
        ),
    )(*args)


def solution(mesh):
    in_specs = (
        P("sp", "tp"), P("sp", "tp"), P(None, "tp"), P("tp"), P("tp"), P("tp"), P(None, "tp"), P("sp", "tp"), P("tp"),
        P("sp", None), P("sp", None), P("sp", None, "tp"), P("sp", None, "tp"), P("sp", None, "tp"),
        P(None, "tp"), P(None, "tp"), P(None, "tp"),
    )
    return jax.shard_map(shards, mesh=mesh, in_specs=in_specs, out_specs=P("sp", "tp"), check_vma=False)
```

time: 169 us -> 129 us (0.76)
  Pallas kernels: 168 us -> 127 us
    pallas_call x1, Pallas kernels: 168 us -> 127 us  [shards(): pl.pallas_call(kernel, name='layer', out_shape=jax.ShapeDtypeStruct((ROWS...]
where the time goes in v2:
time: 129 us
  Pallas kernels  127 us (98%)
  local copies, waits for them, and re-layouts  1.57 us (1%)
    pallas_call x1, Pallas kernels, shards(): pl.pallas_call(kernel, name='layer', out_shape=jax.ShapeDtypeStruct((ROWS...  127 us

profile of v2, /device:TPU:1, one launch (start us, length us, event | category | flops | bytes accessed | tf_op | source)
XLA Modules:
  0.0 128.7 jit_solution(13509163072546105922)
XLA Ops:
  0.0 127.1 %layer.1 = bf16[256,256]{1,0:T(8,128)(2,1)} custom-call(bf16[256,128]{1,0:T(8,128)(2,1)} %u_val.1, bf16[256,128]{1,0:T(8,128)(2,1)} %u_gate.1, f32[31,128]{1,0:T(8,128)} %conv_weight.1, f32[128]{0:T(128)} %conv_bias.1, f32[128]{0:T(128)} %ln_gain.1, f32[128]{0:T(128)} %ln_bias.1, bf16[2048,256]{1,0:T(8,128)(2,1)} %proj.1, bf16[256,256]{1,0:T(8,128)(2,1)} %resid.1, ...), custom_call_target="tpu_custom_call" | custom-call | tf_op jit(solution)/shard_map/layer/pallas_call | solution.py:480
  127.1 1.6 %copy.19 = bf16[256,256]{1,0:T(8,128)(2,1)} copy(bf16[256,256]{1,0:T(8,128)(2,1)} %layer.1) | data formatting | bytes 262144

commit v3 on v2

--- a/solution.py
+++ b/solution.py
@@ -18,7 +18,8 @@
 CAP = 32
 SLOTS = SP * CAP
 CHUNKS = 4
-SENDS, RECVS = 9 + 3 * CHUNKS, 5 + 24 * 3 + CHUNKS * (1 + 3 + 1 + 24)
+HOPS = 4
+SENDS, RECVS = 9 + 3 * CHUNKS, 6 + 24 * 2 + CHUNKS * (2 + 3 + 2 + 24)
 ORDER = (3, 4, 2, 5, 1, 6, 0, 7)
 EPS = 1e-6
 
@@ -87,6 +88,27 @@
     def rounds(self):
         right = self.send(0, 0, 0, 1, 1)
         left = self.send(0, 0, 0, 1, -1)
+        far = self.send(0, 0, 0, 1, 2)
+        two = {0: self.both(0)}
+        yield
+        self.block(right)
+        two[-1] = self.both(-1)
+        self.block(left)
+        two[1] = self.both(1)
+        last = self.copies.landing()
+        self.forward(two, 0, last)
+        self.block(far)
+        two[2] = self.both(2)
+        yield
+        self.forward(two, -1, last)
+        self.forward(two, 1, last)
+        self.forward(two, 2, last)
+        yield
+        arrived(self.buf.at[pl.ds(0, 2)], last)
+
+    def lean(self):
+        right = self.send(0, 0, 0, 1, 1)
+        left = self.send(0, 0, 0, 1, -1)
         two = {0: self.both(0)}
         yield
         self.block(right)
@@ -115,13 +137,14 @@
         self.send(d, 1, 2, 2, -1, last)
 
 
-def gather_plane(copies, buf, rows, y, x):
+def gather_plane(copies, buf, rows, y, x, lean=False):
     out = copies.group(buf.at[pl.ds(0, TP - 1)])
     halves = (
-        RingHalf(copies, out, buf, 0, rows // 2, "x", y, x).rounds(),
-        RingHalf(copies, out, buf, rows // 2, rows // 2, "y", y, x).rounds(),
+        RingHalf(copies, out, buf, 0, rows // 2, "x", y, x),
+        RingHalf(copies, out, buf, rows // 2, rows // 2, "y", y, x),
     )
-    for _ in range(5):
+    halves = [half.lean() if lean else half.rounds() for half in halves]
+    for _ in range(HOPS + lean):
         for half in halves:
             next(half, None)
         yield
@@ -201,10 +224,11 @@
     e_gate, e_up, e_down, s_gate, s_up, s_down,
     out,
     v_val, v_gate, v_cw, v_cb, v_lg, v_lb, v_proj, v_resid, v_ng, v_ids, v_wts,
-    ewt, w2, sgu, w_lo, w_hi, s_lo, s_hi,
+    ewt, w2, sgu, w_relay, w_lo, w_hi, s_lo, s_hi,
     in_sem,
     pad, conv, halo_out, halo_in, stat_out, stat_in, co, rm, ssq_out, ssq_in, na,
-    disp, comb_hi, comb_lo, sent, ya, rs_out, rs_in, hid, shared_out, back_out, back,
+    disp, named_b, place_b, comb_hi, comb_lo, scale_row, scale_out, scale_in,
+    sent, ya, rs_out, rs_relay, rs_mid, rs_in, hid, hid_last, back_out, back,
     send_sem, recv_sem,
 ):
     s, t = lax.axis_index("sp"), lax.axis_index("tp")
@@ -247,12 +271,25 @@
 
     copies = Copies(send_sem, recv_sem)
 
-    spread_out, spread_in = copies.group(w2.at[pl.ds(0, 3)]), copies.landing()
-
-    def spread(k):
-        for n in (2, 1, 3):
-            to = wrap(x + n)
-            copies(ewt.at[SIDE * k + to], w2.at[k, x], {"tp": y * SIDE + to}, spread_out, spread_in)
+    spread_out, spread_in, relay_in = copies.group(w2), copies.landing(), copies.landing()
+    to_right, to_left = {"tp": y * SIDE + wrap(x + 1)}, {"tp": y * SIDE + wrap(x - 1)}
+    sides = ((to_right, 1, (0, 1)), (to_left, -1, (2, 3)))
+
+    def spread_far():
+        for to, step, ks in sides:
+            for k in ks:
+                copies(ewt.at[SIDE * k + wrap(x + 2)], w_relay.at[k], to, spread_out, relay_in)
+
+    def spread_near():
+        phase("spread")
+        for k in range(SIDE):
+            for to, step, ks in sides:
+                copies(ewt.at[SIDE * k + wrap(x + step)], w2.at[k, x], to, spread_out, spread_in)
+        arrived(w_relay, relay_in)
+        for to, step, ks in sides:
+            for k in ks:
+                copies(w_relay.at[k], w2.at[k, wrap(x - step)], to, spread_out, spread_in)
+        yield None
 
     phase("gated")
     for k in (0, 1):
@@ -275,6 +312,9 @@
     ).astype(F32).astype(BF16)
     place = jnp.sum(dot(named.astype(BF16), earlier) * named, axis=0, keepdims=True)
     slot = id_row * CAP + place
+    named_b[...] = named.astype(BF16)
+    slot_in = lax.broadcasted_iota(jnp.int32, (128, 2 * ROWS), 0).astype(F32)
+    place_b[...] = jnp.where(slot_in == place, 1.0, 0.0).astype(BF16)
     slot_0, slot_1 = slot[:, :ROWS], slot[:, ROWS:]
     row = lax.broadcasted_iota(jnp.int32, (SLOTS, ROWS), 0).astype(F32)
     disp[...] = jnp.where((row == slot_0) | (row == slot_1), 1.0, 0.0).astype(BF16)
@@ -293,6 +333,10 @@
     phase("halo")
     halo = copies.landing()
     copies(halo_out, halo_in, {"sp": lax.rem(s + 1, SP)}, copies.group(halo_in), halo)
+    arrived(ewt, in_sem.at[17])
+    spread_far()
+    for k in range(SIDE):
+        w2[k, x] = ewt[SIDE * k + x]
     for k in (2, 3, 4, 5):
         loads[k].wait()
     arrived(halo_in, halo)
@@ -309,12 +353,16 @@
     mean = jnp.sum(mine, axis=1, keepdims=True) * (1.0 / CH)
     off = mine - mean
     stat_out[...] = lanes([mean, jnp.sum(off * off, axis=1, keepdims=True)])[0:8]
+    stat_out[2:3, 0:CH] = v_lg[...].reshape(1, CH)
+    stat_out[3:4, 0:CH] = v_lb[...].reshape(1, CH)
     stats = to_peers(copies, stat_out, stat_in, t)
-    arrived(ewt, in_sem.at[17])
-    spread(0)
-    for k in range(SIDE):
-        w2[k, x] = ewt[SIDE * k + x]
+    co[t] = off.astype(BF16)
+    gather = gather_plane(copies, co, ROWS, y, x)
+    next(gather)
     stat_in[t] = stat_out[...]
+    phase("gather_co0")
+    next(gather)
+    phase("stats_wait")
     arrived(stat_in.at[pl.ds(0, TP - 1)], stats)
     means = stat_in[:, 0, :]
     total_mean = jnp.sum(means, axis=0, keepdims=True) * (1.0 / TP)
@@ -322,30 +370,41 @@
     var = (
         jnp.sum(stat_in[:, 1, :], axis=0, keepdims=True) + CH * jnp.sum(off * off, axis=0, keepdims=True)
     ) * (1.0 / CONV)
-    cols = columns([total_mean, lax.rsqrt(var + EPS)])
-    normed = (mine - cols[:, 0:1]) * cols[:, 1:2]
-    co[t] = silu(normed * v_lg[...].reshape(1, CH) + v_lb[...].reshape(1, CH)).astype(BF16)
-    phase("gather_co")
-    run(gather_plane(copies, co, ROWS, y, x))
-
+    around = [(dy, dx) for dy in (0, 1, 3) for dx in (0, 1, 3)]
+    around += [(2, dx) for dx in range(SIDE)] + [(dy, 2) for dy in (0, 1, 3)]
+    around = [wrap(y + dy) * SIDE + wrap(x + dx) for dy, dx in around]
+    cols = columns([stat_in[k, 0:1, :] - total_mean for k in around] + [lax.rsqrt(var + EPS)])
+    rstd = jnp.broadcast_to(cols[:, TP : TP + 1], (ROWS, CH))
+
+    def normed(n):
+        k = around[n]
+        v = (co[k].astype(F32) + cols[:, n : n + 1]) * rstd
+        return silu(v * stat_in[k, 2:3, 0:CH] + stat_in[k, 3:4, 0:CH]).astype(BF16)
+
+    def projected(n):
+        w = [v_proj[pl.ds(pl.multiple_of(CH * around[m], CH), CH), :] for m in (n, n + 1)]
+        return dot(jnp.concatenate([normed(n), normed(n + 1)], axis=1), jnp.concatenate(w, axis=0))
+
+    phase("gather_co1")
+    next(gather)
     phase("project")
     for k in (8, 9, 10):
         loads[k].wait()
     acc = v_resid[...].astype(F32)
-    for k in range(TP // 2):
-        acc = acc + dot(jnp.concatenate([co[2 * k], co[2 * k + 1]], axis=1), v_proj[pl.ds(256 * k, 256), :])
+    for n in range(0, 8, 2):
+        acc = acc + projected(n)
+    phase("gather_co2")
+    next(gather)
+    phase("project_end")
+    for n in range(8, TP, 2):
+        acc = acc + projected(n)
     mid = acc.astype(BF16)
     rm[...] = mid
     wide = mid.astype(F32)
     ssq_out[...] = lanes([jnp.sum(wide * wide, axis=1, keepdims=True)])[0:8]
-    phase("ssq")
     squares = to_peers(copies, ssq_out, ssq_in, t)
-    spread(1)
     ssq_in[t] = ssq_out[...]
-    arrived(ssq_in.at[pl.ds(0, TP - 1)], squares)
-    scale = lax.rsqrt(jnp.sum(ssq_in[:, 0, :], axis=0, keepdims=True) * (1.0 / D) + EPS)
-    na[t] = (wide * columns([scale])[:, 0:1] * v_ng[...].reshape(1, FEAT)).astype(BF16)
-
+    na[t] = (wide * v_ng[...].reshape(1, FEAT)).astype(BF16)
     phase("dispatch")
     rows = dot(disp[...], na[t]).astype(BF16)
     sent[...] = rows.reshape(SP, CAP, FEAT)
@@ -361,6 +420,30 @@
                 copies(sent.at[e], ya.at[c, y, pl.ds(CAP * j, CAP)], {"sp": e}, moves_out, moves[c])
         yield None
 
+    scales_out = copies.group(scale_out.at[pl.ds(0, SP - 1)])
+    scales = [copies.landing() for c in range(CHUNKS)]
+
+    def rescale():
+        phase("ssq")
+        arrived(ssq_in.at[pl.ds(0, TP - 1)], squares)
+        scale = lax.rsqrt(jnp.sum(ssq_in[:, 0, :], axis=0, keepdims=True) * (1.0 / D) + EPS)
+        scale_row[...] = scale
+        high = scale.astype(BF16)
+        both = jnp.zeros((SP, 128), F32)
+        for n in range(2):
+            at = pl.ds(ROWS * n, ROWS)
+            for part in (high, (scale - high.astype(F32)).astype(BF16)):
+                both = both + dot_t(named_b[:, at] * part, place_b[:, at])
+        scale_out[...] = both.reshape(SP, 1, 128)
+        for c in range(CHUNKS):
+            for j in ORDER:
+                k = CHUNKS * j + c
+                if k:
+                    e = lax.rem(s + SP - k, SP)
+                    copies(scale_out.at[e], scale_in.at[c, j], {"sp": e}, scales_out, scales[c])
+        scale_in[0, 0] = scale_out[s]
+        yield None
+
     ya[0, y, pl.ds(0, CAP), :] = sent[s]
     lane = lax.broadcasted_iota(jnp.int32, (128, 128), 1)
 
@@ -368,38 +451,31 @@
         h = silu(acc) * pltpu.roll(acc, 64, axis=1)
         return jnp.where(lane < 64, h[:128], pltpu.roll(h[128:], 64, axis=1)).astype(BF16)
 
-    def down(c, lo, hi):
+    def down(buf, at, lo, hi):
         both = []
         for ref in (lo, hi):
             acc = jnp.zeros((128, FEAT), F32)
             for k in range(TP // 2):
-                pair = jnp.concatenate([hid[c, 2 * k], hid[c, 2 * k + 1]], axis=1)
+                pair = jnp.concatenate([buf[2 * k, at, :], buf[2 * k + 1, at, :]], axis=1)
                 acc = acc + dot(pair, ref[pl.ds(2 * k, 2)].reshape(2 * 128, FEAT))
             both.append(acc)
         return both
 
-    def more():
-        for k in range(2, 4):
-            spread(k)
-        yield None
-
     def shared():
+        steps = gather_plane(copies, na, ROWS, y, x, lean=True)
+        for n in range(HOPS + 1):
+            phase(f"na{n}")
+            next(steps)
+            yield 6.0 if n else 12.0
         phase("shared")
-        for _ in gather_plane(copies, na, ROWS, y, x):
-            yield 3.0
         for k in (11, 12):
             loads[k].wait()
         acc = jnp.zeros((ROWS, 128), F32)
         for k in range(TP):
             acc = acc + dot_t(na[k], sgu[:, pl.ds(FEAT * k, FEAT)])
-        hid[CHUNKS, t] = hidden(acc)
-        for _ in gather_plane(copies, hid.at[CHUNKS], 128, y, x):
-            yield 4.0
-        ready(downs)
-        lo, hi = down(CHUNKS, s_lo, s_hi)
-        shared_out[pl.ds(0, 128), :] = lo
-        shared_out[pl.ds(128, 128), :] = hi
-
+        hid_last[t, pl.ds(128, 128), :] = hidden(acc * columns([scale_row[...]])[:, 0:1])
+
+    own_rows = shared()
     returns_out, returns = copies.group(back.at[pl.ds(0, SP - 1)]), copies.landing()
 
     def routed(c):
@@ -410,7 +486,7 @@
         up_y, down_y = {"tp": wrap(y + 1) * SIDE + x}, {"tp": wrap(y - 1) * SIDE + x}
         copies(ya.at[c, y], ya.at[c, y], up_y, out, a)
         copies(ya.at[c, y], ya.at[c, y], down_y, out, b)
-        yield 4.5
+        yield 4.8
         phase(f"ya{c}")
         arrived(ya.at[c, 0], a)
         at = ya.at[c, wrap(y - 1), pl.ds(0, 128)]
@@ -418,7 +494,7 @@
         arrived(ya.at[c, 0], b)
         at = ya.at[c, wrap(y + 1), pl.ds(128, 128)]
         copies(at, at, down_y, out, far)
-        yield 3.0
+        yield 4.0
         phase(f"yb{c}")
         arrived(ya.at[c, 0], far)
         if c == 0:
@@ -429,23 +505,48 @@
             acc = acc + dot_t(ya[c, k], w2[k].reshape(4 * 128, FEAT))
         for k in range(SIDE):
             rs_out[c, k] = acc[:, 128 * k : 128 * (k + 1)].astype(BF16)
-        out, parts = copies.group(rs_in.at[c, pl.ds(0, 3)]), copies.landing()
-        for k in (2, 1, 3):
-            to = wrap(x + k)
-            copies(rs_out.at[c, to], rs_in.at[c, x], {"tp": y * SIDE + to}, out, parts)
-        yield 5.0
+        out, relay, parts = copies.group(rs_out.at[c, pl.ds(0, 3)]), copies.landing(), copies.landing()
+        right, left, lo, hi = wrap(x + 1), wrap(x - 1), pl.ds(0, 128), pl.ds(128, 128)
+        to_r, to_l = {"tp": y * SIDE + right}, {"tp": y * SIDE + left}
+        copies(rs_out.at[c, wrap(x + 2), lo], rs_relay.at[c, 0], to_r, out, relay)
+        copies(rs_out.at[c, wrap(x + 2), hi], rs_relay.at[c, 1], to_l, out, relay)
+        copies(rs_out.at[c, right, hi], rs_in.at[c, 0, hi], to_r, out, parts)
+        copies(rs_out.at[c, left, lo], rs_in.at[c, 1, lo], to_l, out, parts)
+        yield 3.5
+        phase(f"relay{c}")
+        arrived(rs_relay.at[c], relay)
+        rs_mid[c, 0] = (rs_out[c, right, lo, :].astype(F32) + rs_relay[c, 0].astype(F32)).astype(BF16)
+        rs_mid[c, 1] = (rs_out[c, left, hi, :].astype(F32) + rs_relay[c, 1].astype(F32)).astype(BF16)
+        copies(rs_mid.at[c, 0], rs_in.at[c, 0, lo], to_r, out, parts)
+        copies(rs_mid.at[c, 1], rs_in.at[c, 1, hi], to_l, out, parts)
+        yield 3.0
         phase(f"rs{c}")
-        arrived(rs_in.at[c, pl.ds(0, 3)], parts)
-        acc = rs_out[c, x].astype(F32)
-        for k in range(1, SIDE):
-            acc = acc + rs_in[c, wrap(x + k)].astype(F32)
-        hid[c, t] = hidden(acc)
-        for n, _ in enumerate(gather_plane(copies, hid.at[c], 128, y, x)):
-            yield 2.6
+        arrived(rs_in.at[c], parts)
+        acc = rs_out[c, x].astype(F32) + rs_in[c, 0].astype(F32) + rs_in[c, 1].astype(F32)
+        first = 0 if c else 1
+        arrived(scale_in.at[c, pl.ds(first, SP // CHUNKS - first)], scales[c])
+        turned = jnp.concatenate(
+            [scale_in[c].reshape(SP // CHUNKS, 128), jnp.zeros((128 - SP // CHUNKS, 128), F32)], axis=0
+        ).T
+        acc = acc * jnp.concatenate(
+            [jnp.broadcast_to(turned[0:CAP, j : j + 1], (CAP, 128)) for j in range(SP // CHUNKS)], axis=0
+        )
+        if c < CHUNKS - 1:
+            buf, rows = hid.at[c], 128
+        else:
+            run(own_rows)
+            phase(f"hid{c}0")
+            buf, rows = hid_last, 256
+        buf[t, pl.ds(0, 128), :] = hidden(acc)
+        steps = gather_plane(copies, buf, rows, y, x)
+        next(steps)
+        for n in range(1, HOPS):
+            yield 3.2
             phase(f"hid{c}{n}")
+            next(steps)
         ready(downs)
         phase(f"down{c}")
-        lo, hi = down(c, w_lo, w_hi)
+        lo, hi = down(buf, pl.ds(0, 128), w_lo, w_hi)
         back_out[c, pl.ds(0, 4)] = lo.astype(BF16).reshape(4, CAP, FEAT)
         back_out[c, pl.ds(4, 4)] = hi.astype(BF16).reshape(4, CAP, FEAT)
         for j in ORDER:
@@ -453,16 +554,18 @@
             if k:
                 copies(back_out.at[c, j], back.at[s], {"sp": lax.rem(s + k, SP)}, returns_out, returns)
 
-    tasks = [(4.5 * c, dispatch(c)) for c in range(CHUNKS)]
-    tasks += [(0.0, more()), (0.1, shared())]
-    tasks += [(10.0 + 4.5 * c, routed(c)) for c in range(CHUNKS)]
+    tasks = [(0.0, dispatch(0)), (0.1, dispatch(1)), (0.2, spread_near()), (2.0, own_rows)]
+    tasks += [(5.0, rescale()), (5.1, dispatch(2)), (5.2, dispatch(3))]
+    tasks += [(at, routed(c)) for c, at in enumerate((8.0, 15.5, 20.0, 26.0))]
     interleave(tasks)
     back[s] = back_out[0, 0]
+    phase("shared_down")
+    own = rm[...].astype(F32) + jnp.concatenate(down(hid_last, pl.ds(128, 128), s_lo, s_hi), axis=0)
     phase("back_wait")
     arrived(back.at[pl.ds(0, SP - 1)], returns)
     phase("combine")
     full = back[...].reshape(SLOTS, FEAT)
-    acc = rm[...].astype(F32) + shared_out[...] + dot(comb_hi[...], full) + dot(comb_lo[...], full)
+    acc = own + dot(comb_hi[...], full) + dot(comb_lo[...], full)
     out[...] = acc.astype(BF16)
     phase("drain")
     copies.drain()
@@ -486,14 +589,16 @@
         scratch_shapes=[
             bf(ROWS, CH), bf(ROWS, CH), f(TAPS, CH), f(CH), f(CH), f(CH), bf(CONV, FEAT), bf(ROWS, FEAT), f(FEAT),
             pltpu.VMEM((2, ROWS), jnp.int32), f(2, ROWS),
-            bf(TP, 128, FEAT), bf(SIDE, SIDE, 128, FEAT), bf(128, D),
+            bf(TP, 128, FEAT), bf(SIDE, SIDE, 128, FEAT), bf(128, D), bf(SIDE, 128, FEAT),
             bf(TP, 128, FEAT), bf(TP, 128, FEAT), bf(TP, 128, FEAT), bf(TP, 128, FEAT),
             pltpu.SemaphoreType.DMA((18,)),
             f(32 + ROWS, CH), f(ROWS, CH), bf(32, CH), bf(32, CH), f(8, ROWS), f(TP, 8, ROWS), bf(TP, ROWS, CH),
             bf(ROWS, FEAT), f(8, ROWS), f(TP, 8, ROWS), bf(TP, ROWS, FEAT),
-            bf(SLOTS, ROWS), bf(ROWS, SLOTS), bf(ROWS, SLOTS),
-            bf(SP, CAP, FEAT), bf(CHUNKS, SIDE, ROWS, FEAT), bf(CHUNKS, SIDE, ROWS, 128), bf(CHUNKS, SIDE, ROWS, 128),
-            bf(CHUNKS + 1, TP, 128, 128), f(ROWS, FEAT), bf(CHUNKS, SP // CHUNKS, CAP, FEAT), bf(SP, CAP, FEAT),
+            bf(SLOTS, ROWS), bf(SP, 2 * ROWS), bf(128, 2 * ROWS), bf(ROWS, SLOTS), bf(ROWS, SLOTS),
+            f(1, ROWS), f(SP, 1, 128), f(CHUNKS, SP // CHUNKS, 1, 128),
+            bf(SP, CAP, FEAT), bf(CHUNKS, SIDE, ROWS, FEAT), bf(CHUNKS, SIDE, ROWS, 128),
+            bf(CHUNKS, 2, 128, 128), bf(CHUNKS, 2, 128, 128), bf(CHUNKS, 2, ROWS, 128),
+            bf(CHUNKS - 1, TP, 128, 128), bf(TP, 256, 128), bf(CHUNKS, SP // CHUNKS, CAP, FEAT), bf(SP, CAP, FEAT),
             pltpu.SemaphoreType.DMA((SENDS,)), pltpu.SemaphoreType.DMA((RECVS,)),
         ],
         compiler_params=pltpu.CompilerParams(

time: 129 us -> 115 us (0.89)
  Pallas kernels: 127 us -> 113 us
    pallas_call x1, Pallas kernels: 127 us -> 113 us  [shards(): pl.pallas_call(kernel, name='layer', out_shape=jax.ShapeDtypeStruct((ROWS...]
where the time goes in v3:
time: 115 us
  Pallas kernels  113 us (98%)
  local copies, waits for them, and re-layouts  1.57 us (1%)
    pallas_call x1, Pallas kernels, shards(): pl.pallas_call(kernel, name='layer', out_shape=jax.ShapeDtypeStruct((ROWS...  113 us

profile of v3, /device:TPU:1, one launch (start us, length us, event | category | flops | bytes accessed | tf_op | source)
XLA Modules:
  0.0 114.8 jit_solution(15099723640519873298)
XLA Ops:
  0.0 113.2 %layer.1 = bf16[256,256]{1,0:T(8,128)(2,1)} custom-call(bf16[256,128]{1,0:T(8,128)(2,1)} %u_val.1, bf16[256,128]{1,0:T(8,128)(2,1)} %u_gate.1, f32[31,128]{1,0:T(8,128)} %conv_weight.1, f32[128]{0:T(128)} %conv_bias.1, f32[128]{0:T(128)} %ln_gain.1, f32[128]{0:T(128)} %ln_bias.1, bf16[2048,256]{1,0:T(8,128)(2,1)} %proj.1, bf16[256,256]{1,0:T(8,128)(2,1)} %resid.1, ...), custom_call_target="tpu_custom_call" | custom-call | tf_op jit(solution)/shard_map/layer/pallas_call | solution.py:583
  113.2 1.6 %copy.19 = bf16[256,256]{1,0:T(8,128)(2,1)} copy(bf16[256,256]{1,0:T(8,128)(2,1)} %layer.1) | data formatting | bytes 262144
